TPU v7x, 32 devices: a whole 2x2x4 slice. The times are simulated.
32 devices in a mesh: sp: 16 (over z, y, x), tp: 2 (over core).
Axes of the slice: x: 2, y: 2, z: 4, core: 2. Of those that a mesh axis runs over, the one named last changes fastest.
Arguments:
- residual: bfloat16 [2048, 4096], P('tp', 'sp'), may hold values from -6 to 6
- values: bfloat16 [4096, 4096], P('sp', 'tp'), may hold values from -6 to 6
- gate_input: bfloat16 [4096, 4096], P('sp', 'tp'), may hold values from -6 to 6
- group_keys: bfloat16 [4096, 3072], P('sp', 'tp'), may hold values from -6 to 6
- time_step: float32 [64, 4096], P('tp', 'sp'), may hold values from -8 to 14
- decay_rate: float32 [64], P('tp'), may hold values from 0 to 2
- skip_gain: float32 [64], P('tp'), may hold values from 0.25 to 2
- conv_values: bfloat16 [4, 4096], P(None, 'tp'), may hold values from -3 to 3
- conv_keys: bfloat16 [4, 3072], P(None, 'tp'), may hold values from -3 to 3
- mix_gain: float32 [4096], P('tp'), may hold values from 0.1 to 1.9
- out_weight: bfloat16 [4096, 2048], P('tp'), may hold values from -0.09375 to 0.09375
- norm_gain: float32 [2048], replicated, may hold values from 0.1 to 1.9
- hidden_gate: bfloat16 [2048, 5120], P('sp', 'tp'), may hold values from -0.125 to 0.125
- hidden_up: bfloat16 [2048, 5120], P('sp', 'tp'), may hold values from -0.125 to 0.125
- hidden_conv: bfloat16 [2, 3, 5120], P(None, None, 'tp'), may hold values from -3.5 to 3.5
- hidden_down: bfloat16 [5120, 2048], P('tp', 'sp'), may hold values from -0.078125 to 0.078125
Outputs:
- layer_out: bfloat16 [2048, 4096], P('tp', 'sp')
All inputs are finite; a program needn't handle non-finite values.
Results may differ from a plain program's by a relative error of at most 0.019.
Values may be sent and summed in bfloat16 or wider, within the bound.
A program may use at most 128 MiB of HBM per device.

v0:
```python
import jax
import jax.numpy as jnp
from jax import lax
from jax.sharding import PartitionSpec as P

GROUP_HEADS = 8
HEAD_SIZE = 64
STATE_WIDE = 128
STATE_NARROW = 64
BLOCK = 128
NORM_FLOOR = 0.1
HIGHEST = lax.Precision.HIGHEST


def from_behind(value, axis, steps):
    count = lax.axis_size(axis)
    first, last = (max(0, -steps), min(count, count - steps))
    return lax.ppermute(value, axis, [(source, source + steps) for source in range(first, last)])


def prefix(shard, axis, join, neutral):
    place = lax.axis_index(axis)
    gathered = jax.tree.map(
        lambda a, kind: lax.all_gather(a.astype(kind), axis),
        shard,
        (jnp.bfloat16, jnp.bfloat16, jnp.bfloat16, jnp.bfloat16),
    )
    state = jax.tree.map(lambda a, e: jnp.zeros_like(a) + jnp.asarray(e, a.dtype), shard, neutral)

    def one(lap, state):
        return join(
            state,
            jax.tree.map(
                lambda a, own: lax.dynamic_index_in_dim(a, lap, 0, False).astype(own.dtype),
                gathered,
                shard,
            ),
        )

    return lax.fori_loop(0, place, one, state)


def from_partner_2(shard, axis, stride):
    return lax.ppermute(shard, axis, [(i, i ^ 1 << stride) for i in range(lax.axis_size(axis))])


def tap_sum(joined, weights, row_count):
    summed = weights[0].astype(jnp.float32) * joined[0:row_count]
    for tap_index in range(1, weights.shape[0]):
        summed = (
            summed
            + weights[tap_index].astype(jnp.float32) * joined[tap_index : tap_index + row_count]
        )
    return summed


def block_heads(inputs, in_keys, out_keys, deltas, decay_rates, skip_table, carried):
    length = inputs.shape[0]
    running = jnp.cumsum(-decay_rates * deltas, axis=0)
    weighted = inputs * deltas[..., None]
    scores = jnp.einsum("ign,jgn->gij", out_keys, in_keys, precision=HIGHEST)
    by_head = jnp.transpose(running, (1, 2, 0))
    between = by_head[..., :, None] - by_head[..., None, :]
    lower_mask = jnp.tril(jnp.ones((length, length), dtype=bool))
    decays = jnp.exp(jnp.where(lower_mask, between, -jnp.inf))
    inside = jnp.einsum("ghij,jghp->ighp", scores[:, None] * decays, weighted, precision=HIGHEST)
    carried_part = (
        jnp.einsum("ign,ghpn->ighp", out_keys, carried, precision=HIGHEST)
        * jnp.exp(running)[..., None]
    )
    to_end = jnp.exp(by_head[..., -1:] - by_head)
    fresh_state = jnp.einsum("jgn,ghj,jghp->ghpn", in_keys, to_end, weighted, precision=HIGHEST)
    updated = carried * jnp.exp(by_head[..., -1])[..., None, None] + fresh_state
    return (inside + carried_part + inputs * skip_table[..., None], updated)


def contract_rows(left, right):
    return lax.dot_general(
        left, right, (((0,), (0,)), ((), ())), preferred_element_type=jnp.float32
    )


def combine_states(first_part, second_part):
    return (
        first_part[0] * second_part[0],
        first_part[1] * second_part[0][..., None, None] + second_part[1],
        first_part[2] * second_part[2],
        first_part[3] * second_part[2][..., None, None] + second_part[3],
    )


def hidden_taps(both_pre, edge_cols, taps, row_count):
    joined_hidden = jnp.concatenate([edge_cols, both_pre], axis=2).astype(jnp.float32)
    conv_total = taps[:, 0, :, None].astype(jnp.float32) * joined_hidden[:, :, 0:row_count]
    for tap_index in range(1, taps.shape[1]):
        conv_total = (
            conv_total
            + taps[:, tap_index, :, None].astype(jnp.float32)
            * joined_hidden[:, :, tap_index : tap_index + row_count]
        )
    return (jax.nn.silu(conv_total[0]) * conv_total[1]).astype(jnp.bfloat16)


def local(
    residual,
    values,
    gate_input,
    group_keys,
    time_step,
    decay_rate,
    skip_gain,
    conv_values,
    conv_keys,
    mix_gain,
    out_weight,
    norm_gain,
    hidden_gate,
    hidden_up,
    hidden_conv,
    hidden_down,
):
    row_count = values.shape[0]
    value_cols = values.shape[1]
    tap_count = conv_values.shape[0]
    tail_rows = jnp.concatenate(
        [values[row_count - tap_count + 1 :], group_keys[row_count - tap_count + 1 :]], axis=1
    )
    before_rows = from_behind(tail_rows, "sp", 1)
    joined_values = jnp.concatenate([before_rows[:, :value_cols], values], axis=0).astype(
        jnp.float32
    )
    joined_keys = jnp.concatenate([before_rows[:, value_cols:], group_keys], axis=0).astype(
        jnp.float32
    )
    group_count = group_keys.shape[1] // (2 * STATE_WIDE + 2 * STATE_NARROW)
    inputs = jax.nn.silu(tap_sum(joined_values, conv_values, row_count)).reshape(
        row_count, group_count, GROUP_HEADS, HEAD_SIZE
    )
    key_rows = jax.nn.silu(tap_sum(joined_keys, conv_keys, row_count)).reshape(
        row_count, group_count, -1
    )
    deltas = jax.nn.softplus(time_step).T.reshape(row_count, group_count, GROUP_HEADS)
    rate_table = decay_rate.reshape(group_count, GROUP_HEADS)
    skip_table = skip_gain.reshape(group_count, GROUP_HEADS)
    running = jnp.cumsum(-rate_table * deltas, axis=0)
    half_heads = GROUP_HEADS // 2
    wide_end = 2 * STATE_WIDE

    def run_kind(head_first, head_last, key_first, state_width):
        in_keys = key_rows[..., key_first : key_first + state_width]
        out_keys = key_rows[..., key_first + state_width : key_first + 2 * state_width]
        carried = jnp.zeros(
            (group_count, head_last - head_first, HEAD_SIZE, state_width), jnp.float32
        )
        block_outs = []
        for block_index in range(row_count // BLOCK):
            row_first = block_index * BLOCK
            row_last = row_first + BLOCK
            block_out, carried = block_heads(
                inputs[row_first:row_last, :, head_first:head_last],
                in_keys[row_first:row_last],
                out_keys[row_first:row_last],
                deltas[row_first:row_last, :, head_first:head_last],
                rate_table[:, head_first:head_last],
                skip_table[:, head_first:head_last],
                carried,
            )
            block_outs.append(block_out)
        return (jnp.concatenate(block_outs, axis=0), carried, out_keys)

    wide_local, wide_state, wide_keys = run_kind(0, half_heads, 0, STATE_WIDE)
    narrow_local, narrow_state, narrow_keys = run_kind(
        half_heads, GROUP_HEADS, wide_end, STATE_NARROW
    )
    span_decay = jnp.exp(running[-1])
    start_value = (
        jnp.ones_like(span_decay[:, :half_heads]),
        jnp.zeros_like(wide_state),
        jnp.ones_like(span_decay[:, half_heads:]),
        jnp.zeros_like(narrow_state),
    )
    incoming = prefix(
        (span_decay[:, :half_heads], wide_state, span_decay[:, half_heads:], narrow_state),
        "sp",
        combine_states,
        start_value,
    )
    growth = jnp.exp(running)[..., None]
    wide_out = (
        wide_local
        + jnp.einsum("ign,ghpn->ighp", wide_keys, incoming[1], precision=HIGHEST)
        * growth[:, :, :half_heads]
    )
    narrow_out = (
        narrow_local
        + jnp.einsum("ign,ghpn->ighp", narrow_keys, incoming[3], precision=HIGHEST)
        * growth[:, :, half_heads:]
    )
    mixer_out = jnp.concatenate([wide_out, narrow_out], axis=2).reshape(row_count, value_cols)
    gated_out = mixer_out * jax.nn.silu(gate_input.astype(jnp.float32))
    squares = lax.psum(jnp.sum(gated_out * gated_out, axis=1), "tp")
    inverse_rms = lax.rsqrt(squares / (value_cols * lax.axis_size("tp")) + NORM_FLOOR)
    normed = (gated_out * inverse_rms[:, None] * mix_gain).astype(jnp.bfloat16)
    mixer_sum = lax.psum_scatter(
        lax.dot_general(
            out_weight, normed, (((0,), (1,)), ((), ())), preferred_element_type=jnp.float32
        ).astype(jnp.bfloat16),
        "tp",
        scatter_dimension=0,
        tiled=True,
    ).astype(jnp.float32)
    own_merged = (residual.astype(jnp.float32) + mixer_sum).astype(jnp.bfloat16)
    merged = lax.all_gather(own_merged, "tp", axis=0, tiled=True)
    merged_wide = merged.astype(jnp.float32)
    inverse_norm = lax.rsqrt(jnp.mean(merged_wide * merged_wide, axis=0) + NORM_FLOOR)
    lifted = (merged_wide * inverse_norm[None, :] * norm_gain[:, None]).astype(jnp.bfloat16)
    hidden_cols = hidden_gate.shape[1]
    edge_taps = hidden_conv.shape[1]
    half_cols = hidden_cols // 2
    parity = lax.axis_index("sp") % 2
    first_member = parity == 0
    sp_count = lax.axis_size("sp")
    weight_rows = hidden_gate.shape[0]
    gate_tiles = jnp.tile(
        jnp.stack([hidden_gate[:, :half_cols], hidden_gate[:, half_cols:]]), (sp_count // 2, 1, 1)
    )
    up_tiles = jnp.tile(
        jnp.stack([hidden_up[:, :half_cols], hidden_up[:, half_cols:]]), (sp_count // 2, 1, 1)
    )
    gate_half, up_half = (
        lax.all_to_all(gate_tiles, "sp", split_axis=0, concat_axis=0, tiled=True),
        lax.all_to_all(up_tiles, "sp", split_axis=0, concat_axis=0, tiled=True),
    )
    gate_half = gate_half.reshape(sp_count * weight_rows, half_cols)
    up_half = up_half.reshape(sp_count * weight_rows, half_cols)
    partner_lifted = from_partner_2(lifted, "sp", 0)
    pair_lifted = jnp.where(
        first_member,
        jnp.concatenate([lifted, partner_lifted], axis=1),
        jnp.concatenate([partner_lifted, lifted], axis=1),
    )
    pair_count = 2 * row_count
    pair_pre = jnp.stack(
        [contract_rows(gate_half, pair_lifted), contract_rows(up_half, pair_lifted)]
    ).astype(jnp.bfloat16)
    pair_edge = from_behind(pair_pre[:, :, pair_count - edge_taps + 1 :], "sp", 2)
    half_taps = lax.dynamic_slice_in_dim(hidden_conv, parity * half_cols, half_cols, 2)
    half_hidden = hidden_taps(pair_pre, pair_edge, half_taps, pair_count)
    own_part = lax.dynamic_slice_in_dim(half_hidden, parity * row_count, row_count, 1)
    for_partner = lax.dynamic_slice_in_dim(half_hidden, (1 - parity) * row_count, row_count, 1)
    from_partner = from_partner_2(for_partner, "sp", 0)
    hidden = jnp.where(
        first_member,
        jnp.concatenate([own_part, from_partner], axis=0),
        jnp.concatenate([from_partner, own_part], axis=0),
    )
    down_whole = lax.all_gather(hidden_down, "sp", axis=1, tiled=True)
    hidden_sum = lax.psum_scatter(
        contract_rows(down_whole, hidden).astype(jnp.bfloat16),
        "tp",
        scatter_dimension=0,
        tiled=True,
    ).astype(jnp.float32)
    return (own_merged.astype(jnp.float32) + hidden_sum).astype(jnp.bfloat16)


def solution(mesh):
    in_specs = (
        P("tp", "sp"),
        P("sp", "tp"),
        P("sp", "tp"),
        P("sp", "tp"),
        P("tp", "sp"),
        P("tp"),
        P("tp"),
        P(None, "tp"),
        P(None, "tp"),
        P("tp"),
        P("tp", None),
        P(),
        P("sp", "tp"),
        P("sp", "tp"),
        P(None, None, "tp"),
        P("tp", "sp"),
    )
    out_specs = P("tp", "sp")
    return jax.shard_map(local, mesh=mesh, in_specs=in_specs, out_specs=out_specs, check_vma=False)
```

profile of v0, /device:TPU:0, one launch (start us, length us, event | category | flops | bytes accessed | tf_op | source)
XLA Modules:
  0.0 622.7 jit_solution(8149238865578526616)
XLA Ops:
  6.5 0.8 slice.219
  7.4 0.8 slice.220
  8.2 4.9 collective-permute-start
  13.0 0.7 reshape.158
  13.9 0.8 fusion.129
  15.7 1.2 copy.125
  17.7 1.2 divide_multiply_fusion
  19.0 1.9 copy.123
  20.9 1.6 maximum_convert_fusion.1
  22.5 2.4 divide_multiply_fusion.1
  24.9 0.6 convolution_add_fusion.1
  25.5 1.3 fusion.44
  28.5 1.7 convolution_add_fusion.3
  30.2 2.5 fusion.43
  32.7 1.1 slice_bitcast_fusion.7
  33.9 2.8 tile.8
  36.6 6.0 all-to-all-start
  42.7 1.8 exp.125
  44.5 1.0 copy.135
  45.5 0.8 exp.120
  46.4 0.8 exp.141
  47.6 2.3 reduce-window.6
  50.1 1.0 copy.138
  51.3 1.1 copy.152
  52.9 125.0 %all-gather.4 = bf16[16,4,4]{2,1,0:T(4,128)(2,1)S(1)} all-gather(bf16[1,4,4]{2,1,0:T(4,128)(2,1)S(1)} %get-tuple-element.151), channel_id=2, replica_groups=mesh['sp'=16,'tp'=2] {'sp'}, dimensions={0}, use_global_device_ids=true | all-gather | bytes 544 | tf_op jit(solution)/shard_map/all_gather | solution.py:24
  177.9 77.3 %all-gather.5 = bf16[16,4,4]{2,1,0:T(4,128)(2,1)S(1)} all-gather(bf16[1,4,4]{2,1,0:T(4,128)(2,1)S(1)} %get-tuple-element.150), channel_id=4, replica_groups=mesh['sp'=16,'tp'=2] {'sp'}, dimensions={0}, use_global_device_ids=true | all-gather | bytes 544 | tf_op jit(solution)/shard_map/all_gather | solution.py:24
  255.4 0.6 fusion.120
  256.0 0.6 fusion.123
  257.1 0.6 fusion.105
  257.8 0.6 fusion.110
  259.5 0.6 fusion.40
  260.1 2.2 fusion.36
  262.3 3.0 fusion.38
  265.3 2.9 fusion.32
  268.3 3.0 fusion.34
  271.6 2.2 fusion.24
  273.8 1.0 fusion.22
  274.8 1.6 pad_maximum_fusion
  276.4 2.0 copy.153
  278.5 0.8 multiply_reduce_fusion
  279.2 2.5 psum.7
  281.7 7.0 %fusion.6 = bf16[2048,256]{0,1:T(8,128)(2,1)} fusion(bf16[2048,2048]{1,0:T(8,128)(2,1)} %param.28, f32[2048]{0:T(1024)S(1)} %copy-done.19, f32[256]{0:T(256)S(1)} %add_rsqrt_fusion.1, f32[256,2048]{1,0:T(8,128)S(1)} %copy.153, bf16[256,2048]{1,0:T(8,128)(2,1)S(1)} %copy-done.5), kind=kOutput, calls=%fused_computation.24 | convolution fusion | flops 2152726528 | bytes 12592128 | tf_op jit(solution)/shard_map/dot_general | solution.py:205
  288.8 1.3 copy.122
  290.1 36.7 %reduce-scatter.3.cloned.1.call-done = bf16[1024,256]{0,1:T(8,128)(2,1)} async-done(((bf16[2048,256]{0,1:T(8,128)(2,1)}), bf16[1024,256]{0,1:T(8,128)(2,1)}) %reduce-scatter.3.cloned.1.call-update) | async-done | bytes 524304 | tf_op jit(solution)/shard_map/reduce_scatter | solution.py:204
  326.8 2.0 add_convert_fusion.1
  329.6 2.8 tile.20
  332.4 6.9 %all-to-all-start.1 = ((bf16[16,128,1280]{2,1,0:T(8,128)(2,1)}), bf16[16,128,1280]{2,1,0:T(8,128)(2,1)}, u32[]{:S(2)}, u32[]{:S(2)}) async-start(bf16[16,128,1280]{2,1,0:T(8,128)(2,1)} %bitcast.260), calls=%async_computation.2 | async-start | bytes 10485760 | tf_op jit(solution)/shard_map/all_to_all | solution.py:232
  339.5 1.5 fusion.12
  341.0 1.5 fusion.14
  342.5 1.9 collective-permute-start.1
  344.5 55.0 %collective-permute-done.1 = bf16[2048,256]{0,1:T(8,128)(2,1)S(1)} collective-permute-done((bf16[2048,256]{0,1:T(8,128)(2,1)S(1)}, bf16[2048,256]{0,1:T(8,128)(2,1)S(1)}, u32[]{:S(2)}, u32[]{:S(2)}) %collective-permute-start.1) | collective-permute-done | bytes 1048608 | tf_op jit(solution)/shard_map/ppermute | solution.py:44
  399.5 5.7 fusion.2
  405.2 75.9 %all-to-all-done.1 = bf16[16,128,1280]{2,1,0:T(8,128)(2,1)} async-done(((bf16[16,128,1280]{2,1,0:T(8,128)(2,1)}), bf16[16,128,1280]{2,1,0:T(8,128)(2,1)}, u32[]{:S(2)}, u32[]{:S(2)}) %all-to-all-start.1) | async-done | bytes 5242912 | tf_op jit(solution)/shard_map/all_to_all | solution.py:232
  481.1 6.7 %fusion.3 = bf16[1,1280,512]{1,2,0:T(8,128)(2,1)S(1)} fusion(bf16[2048,1280]{1,0:T(8,128)(2,1)} %bitcast.75, bf16[2048,256]{0,1:T(8,128)(2,1)} %copy-done.18, bf16[2048,256]{0,1:T(8,128)(2,1)} %copy-done.7, pred[]{:T(512)S(6)} %eq.5), kind=kOutput, calls=%fused_computation.12 | convolution fusion | flops 2694447104 | bytes 8650753 | tf_op jit(solution)/shard_map/dot_general | solution.py:78
  487.8 10.7 %collective-permute-start.2 = (bf16[2,1280,2]{1,2,0:T(2,128)(2,1)S(1)}, bf16[2,1280,2]{1,2,0:T(2,128)(2,1)S(1)}, u32[]{:S(2)}, u32[]{:S(2)}) collective-permute-start(bf16[2,1280,2]{1,2,0:T(2,128)(2,1)S(1)} %pad_maximum_fusion.4), channel_id=1, source_target_pairs={{0,4},{2,6},{4,8},{6,10},{8,12},{10,14},{12,16},{14,18},{16,20},{1... | collective-permute-start | bytes 30728 | tf_op jit(solution)/shard_map/ppermute | solution.py:18
  498.6 1.1 collective-permute-done.2
  500.2 1.6 fusion
  501.8 0.8 fusion.5
  502.8 30.5 %collective-permute-done.3 = bf16[1280,256]{0,1:T(8,128)(2,1)S(1)} collective-permute-done((bf16[1280,256]{0,1:T(8,128)(2,1)S(1)}, bf16[1280,256]{0,1:T(8,128)(2,1)S(1)}, u32[]{:S(2)}, u32[]{:S(2)}) %collective-permute-start.3) | collective-permute-done | bytes 655392 | tf_op jit(solution)/shard_map/ppermute | solution.py:44
  533.3 59.3 %all-gather.13.cloned.1.call-done = bf16[2560,2048]{1,0:T(8,128)(2,1)} async-done(((bf16[2560,128]{1,0:T(8,128)(2,1)}), bf16[2560,2048]{1,0:T(8,128)(2,1)}) %all-gather.13.cloned.1.call-update) | async-done | bytes 10485776 | tf_op jit(solution)/shard_map/all_gather | solution.py:257
  592.6 7.9 %fusion.7 = bf16[2048,256]{0,1:T(8,128)(2,1)} fusion(bf16[2560,2048]{1,0:T(8,128)(2,1)} %all-gather.13.cloned.1.call-done, bf16[1280,256]{0,1:T(8,128)(2,1)S(1)} %collective-permute-done.3, bf16[1280,256]{0,1:T(8,128)(2,1)S(1)} %get-tuple-element.121, pred[]{:T(512)S(6)} %eq.5), kind=kOutput, calls=%fused_computation.25 | convolution fusion | flops 2690777088 | bytes 12845057 | tf_op jit(solution)/shard_map/dot_general | solution.py:78
  600.5 12.9 %reduce-scatter.5.cloned.1.call-done = bf16[1024,256]{0,1:T(8,128)(2,1)} async-done(((bf16[2048,256]{0,1:T(8,128)(2,1)}), bf16[1024,256]{0,1:T(8,128)(2,1)}) %reduce-scatter.5.cloned.1.call-update) | async-done | bytes 524304 | tf_op jit(solution)/shard_map/reduce_scatter | solution.py:258
  613.4 1.2 add_convert_fusion
  614.7 1.0 copy.154
  (125 shorter events, 8.8 us)
Async XLA Ops:
  6.5 9.2 %copy-start.8 = (bf16[256,1536]{1,0:T(8,128)(2,1)S(1)}, bf16[256,1536]{1,0:T(8,128)(2,1)}, u32[]{:S(2)}) copy-start(bf16[256,1536]{1,0:T(8,128)(2,1)} %param.21) | copy-start | bytes 2359300
  6.5 9.0 %copy-start.13 = (bf16[4,2048]{1,0:T(4,128)(2,1)S(1)}, bf16[4,2048]{1,0:T(4,128)(2,1)}, u32[]{:S(2)}) copy-start(bf16[4,2048]{1,0:T(4,128)(2,1)} %param.25) | copy-start | bytes 49156
  6.5 9.1 %copy-start.14 = (bf16[4,1536]{1,0:T(4,128)(2,1)S(1)}, bf16[4,1536]{1,0:T(4,128)(2,1)}, u32[]{:S(2)}) copy-start(bf16[4,1536]{1,0:T(4,128)(2,1)} %param.26) | copy-start | bytes 36868
  6.5 264.8 %all-gather.17.cloned.1.call-start = ((), (), s32[]{:S(2)}) async-start(), calls=%async_computation.9 | async-start | bytes 4456448 | tf_op jit(solution)/shard_map/all_gather | solution.py:24
  8.2 8.9 %collective-permute-start = (bf16[3,3584]{1,0:T(4,128)(2,1)S(1)}, bf16[3,3584]{1,0:T(4,128)(2,1)S(1)}, u32[]{:S(2)}, u32[]{:S(2)}) collective-permute-start(bf16[3,3584]{1,0:T(4,128)(2,1)S(1)} %pad_maximum_fusion.3), channel_id=1, source_target_pairs={{0,2},{2,4},{4,6},{6,8},{8,10},{10,12},{12,14},{14,16},{16,18},{18... | collective-permute-start | bytes 64520 | tf_op jit(solution)/shard_map/ppermute | solution.py:18
  15.2 2.2 copy-start.4
  22.5 2.4 copy-start
  26.9 244.4 %all-gather.15.cloned.1.call-start = ((), (), s32[]{:S(2)}) async-start(), calls=%async_computation.8 | async-start | bytes 4456448 | tf_op jit(solution)/shard_map/all_gather | solution.py:24
  27.8 0.7 copy-start.3
  36.6 292.9 %all-to-all-start = ((bf16[16,128,1280]{2,1,0:T(8,128)(2,1)}), bf16[16,128,1280]{2,1,0:T(8,128)(2,1)}, u32[]{:S(2)}, u32[]{:S(2)}) async-start(bf16[16,128,1280]{2,1,0:T(8,128)(2,1)} %bitcast.259), calls=%async_computation.1 | async-start | bytes 10485760 | tf_op jit(solution)/shard_map/all_to_all | solution.py:231
  42.6 4.9 copy-start.12
  42.6 8.5 %copy-start.17 = (f32[32]{0:T(128)S(1)}, f32[32]{0:T(128)}, u32[]{:S(2)}) copy-start(f32[32]{0:T(128)} %param.24) | copy-start | bytes 388
  42.7 284.1 %reduce-scatter.3.cloned.1.call-start = ((), (), s32[]{:S(2)}) async-start(), calls=%async_computation.4 | async-start | bytes 1572864 | tf_op jit(solution)/shard_map/reduce_scatter | solution.py:204
  46.4 4.8 copy-start.6
  257.7 2.4 copy-start.1
  271.6 2.2 copy-start.10
  271.6 2.2 copy-start.11
  276.4 2.0 copy-start.5
  278.5 3.3 copy-start.19
  288.7 40.7 %copy-start.9 = (bf16[128,2560]{1,0:T(8,128)(2,1)S(1)}, bf16[128,2560]{1,0:T(8,128)(2,1)}, u32[]{:S(2)}) copy-start(bf16[128,2560]{1,0:T(8,128)(2,1)} %param.31) | copy-start | bytes 1966084
  288.7 50.7 %all-gather.11.cloned.1.call-start = ((), (), s32[]{:S(2)}) async-start(), calls=%async_computation.5 | async-start | bytes 1572864 | tf_op jit(solution)/shard_map/all_gather | solution.py:213
  328.9 263.7 %all-gather.13.cloned.1.call-start = ((), (), s32[]{:S(2)}) async-start(), calls=%async_computation.6 | async-start | bytes 11141120 | tf_op jit(solution)/shard_map/all_gather | solution.py:257
  332.4 8.6 %copy-start.15 = (f32[2048]{0:T(1024)S(1)}, f32[2048]{0:T(1024)}, u32[]{:S(2)}) copy-start(f32[2048]{0:T(1024)} %param.29) | copy-start | bytes 24580
  332.4 148.7 %all-to-all-start.1 = ((bf16[16,128,1280]{2,1,0:T(8,128)(2,1)}), bf16[16,128,1280]{2,1,0:T(8,128)(2,1)}, u32[]{:S(2)}, u32[]{:S(2)}) async-start(bf16[16,128,1280]{2,1,0:T(8,128)(2,1)} %bitcast.260), calls=%async_computation.2 | async-start | bytes 10485760 | tf_op jit(solution)/shard_map/all_to_all | solution.py:232
  339.4 274.0 %reduce-scatter.5.cloned.1.call-start = ((), (), s32[]{:S(2)}) async-start(), calls=%async_computation.7 | async-start | bytes 1572864 | tf_op jit(solution)/shard_map/reduce_scatter | solution.py:258
  342.5 62.7 %copy-start.7 = (bf16[2048,256]{0,1:T(8,128)(2,1)}, bf16[2048,256]{0,1:T(8,128)(2,1)S(1)}, u32[]{:S(2)}) copy-start(bf16[2048,256]{0,1:T(8,128)(2,1)S(1)} %fusion.14) | copy-start | bytes 3145732
  342.5 56.9 %collective-permute-start.1 = (bf16[2048,256]{0,1:T(8,128)(2,1)S(1)}, bf16[2048,256]{0,1:T(8,128)(2,1)S(1)}, u32[]{:S(2)}, u32[]{:S(2)}) collective-permute-start(bf16[2048,256]{0,1:T(8,128)(2,1)S(1)} %fusion.14), channel_id=1, source_target_pairs={{0,2},{2,0},{4,6},{6,4},{8,10},{10,8},{12,14},{14,12},{16,18},{18,... | collective-permute-start | bytes 3145736 | tf_op jit(solution)/shard_map/ppermute | solution.py:44
  399.5 5.8 copy-start.18
  487.8 10.8 %copy-start.16 = (bf16[2,3,2560]{2,0,1:T(2,128)(2,1)S(1)}, bf16[2,3,2560]{2,0,1:T(2,128)(2,1)}, u32[]{:S(2)}) copy-start(bf16[2,3,2560]{2,0,1:T(2,128)(2,1)} %param.32) | copy-start | bytes 92164
  487.8 11.9 %collective-permute-start.2 = (bf16[2,1280,2]{1,2,0:T(2,128)(2,1)S(1)}, bf16[2,1280,2]{1,2,0:T(2,128)(2,1)S(1)}, u32[]{:S(2)}, u32[]{:S(2)}) collective-permute-start(bf16[2,1280,2]{1,2,0:T(2,128)(2,1)S(1)} %pad_maximum_fusion.4), channel_id=1, source_target_pairs={{0,4},{2,6},{4,8},{6,10},{8,12},{10,14},{12,16},{14,18},{16,20},{1... | collective-permute-start | bytes 30728 | tf_op jit(solution)/shard_map/ppermute | solution.py:18
  502.7 30.6 %collective-permute-start.3 = (bf16[1280,256]{0,1:T(8,128)(2,1)S(1)}, bf16[1280,256]{0,1:T(8,128)(2,1)S(1)}, u32[]{:S(2)}, u32[]{:S(2)}) collective-permute-start(bf16[1280,256]{0,1:T(8,128)(2,1)S(1)} %get-tuple-element.122), channel_id=1, source_target_pairs={{0,2},{2,0},{4,6},{6,4},{8,10},{10,8},{12,14},{14,12},{16,18},{18,... | collective-permute-start | bytes 1966088 | tf_op jit(solution)/shard_map/ppermute | solution.py:44
  592.6 20.9 %copy-start.2 = (bf16[1024,256]{0,1:T(8,128)(2,1)S(1)}, bf16[1024,256]{0,1:T(8,128)(2,1)}, u32[]{:S(2)}) copy-start(bf16[1024,256]{0,1:T(8,128)(2,1)} %add_convert_fusion.1) | copy-start | bytes 1572868
Sparse Core Ops, SparseCore 0:
  27.0 157.4 all-gather.16
  187.2 74.3 all-gather.14
  288.8 37.9 reduce-scatter.2
  329.0 10.1 all-gather.10
  341.7 250.7 all-gather.12
  600.6 12.7 reduce-scatter.4
where the time goes:
time: 632 us; the launch traced here: 623 us
  waiting for transfers between devices  272 us (43%)
  blocking collectives  205 us (32%)
  matrix products  52.4 us (8%)
  starting transfers between devices  30.7 us (5%)
  local copies, waits for them, and re-layouts  26.2 us (4%)
  other arithmetic  21.9 us (3%)
  between operations  14.4 us (2%)
    all_gather x2, blocking collectives, prefix(): lax.all_gather(a.astype(kind), axis)  202 us
    ppermute x2, waiting for transfers between devices, from_partner_2(): lax.ppermute(shard, axis, [(i, i ^ 1 << stride) for i in range(lax.axis_s...  85.5 us
    all_to_all x1, waiting for transfers between devices, local(): lax.all_to_all(up_tiles, 'sp', split_axis=0, concat_axis=0, tiled=True)  75.9 us
    all_gather x1, waiting for transfers between devices, local(): down_whole = lax.all_gather(hidden_down, 'sp', axis=1, tiled=True)  59.3 us
    reduce_scatter x1, waiting for transfers between devices, local(): lax.psum_scatter(lax.dot_general(out_weight, normed, (((0,), (1,)), ((),...  36.7 us
    dot_general x3, matrix products, contract_rows(): lax.dot_general(left, right, (((0,), (0,)), ((), ())), preferred_element_...  20.3 us
    ppermute x2, starting transfers between devices, from_behind(): lax.ppermute(value, axis, [(source, source + steps) for source in range(f...  15.6 us
    reduce_scatter x1, waiting for transfers between devices, local(): lax.psum_scatter(contract_rows(down_whole, hidden).astype(jnp.bfloat16),...  12.9 us
  transfers between devices with their start and end apart: 12, of which 7 were waited for; matrix products, arithmetic and copies ran while one was open for 13% of the time, Pallas kernels for 0%

commit v1 on v0

--- a/solution.py
+++ b/solution.py
@@ -2,6 +2,7 @@
 import jax.numpy as jnp
 from jax import lax
 from jax.sharding import PartitionSpec as P
+from jax.lax import all_gather
 
 GROUP_HEADS = 8
 HEAD_SIZE = 64
@@ -254,7 +255,8 @@
         jnp.concatenate([own_part, from_partner], axis=0),
         jnp.concatenate([from_partner, own_part], axis=0),
     )
-    down_whole = lax.all_gather(hidden_down, "sp", axis=1, tiled=True)
+    val2 = all_gather(hidden_down, axis_name="sp")
+    down_whole = jnp.concatenate(val2, 1)
     hidden_sum = lax.psum_scatter(
         contract_rows(down_whole, hidden).astype(jnp.bfloat16),
         "tp",

time: 632 us -> 610 us (0.965)
  waiting for transfers between devices: 272 us -> 233 us
  local copies, waits for them, and re-layouts: 26.2 us -> 40 us
    ppermute x2, waiting for transfers between devices: 85.5 us -> 39.2 us  [from_partner_2(): lax.ppermute(shard, axis, [(i, i ^ 1 << stride) for i in range(lax.axis_s...]
    all_to_all x1, waiting for transfers between devices: 75.9 us -> 90.7 us  [local(): lax.all_to_all(up_tiles, 'sp', split_axis=0, concat_axis=0, tiled=True)]
    reshape x0 -> x1, local copies, waits for them, and re-layouts: none -> 13.8 us  [local(): down_whole = jnp.concatenate(val2, 1)]
  transfers between devices with their start and end apart: 12 -> 12, of which waited for: 7 -> 6; matrix products, arithmetic and copies ran while one was open for 13% -> 16% of each run, Pallas kernels for 0% -> 0%
where the time goes in v1:
time: 610 us; the launch traced here: 601 us
  waiting for transfers between devices  233 us (38%)
  blocking collectives  205 us (34%)
  matrix products  52.4 us (9%)
  local copies, waits for them, and re-layouts  40 us (7%)
  starting transfers between devices  33.3 us (5%)
  other arithmetic  22.8 us (4%)
  between operations  14.4 us (2%)
    all_gather x2, blocking collectives, prefix(): lax.all_gather(a.astype(kind), axis)  202 us
    all_to_all x1, waiting for transfers between devices, local(): lax.all_to_all(up_tiles, 'sp', split_axis=0, concat_axis=0, tiled=True)  90.7 us
    all_gather x1, waiting for transfers between devices, local(): val2 = all_gather(hidden_down, axis_name='sp')  57 us
    ppermute x2, waiting for transfers between devices, from_partner_2(): lax.ppermute(shard, axis, [(i, i ^ 1 << stride) for i in range(lax.axis_s...  39.2 us
    reduce_scatter x1, waiting for transfers between devices, local(): lax.psum_scatter(lax.dot_general(out_weight, normed, (((0,), (1,)), ((),...  36.7 us
    dot_general x3, matrix products, contract_rows(): lax.dot_general(left, right, (((0,), (0,)), ((), ())), preferred_element_...  20.3 us
    ppermute x2, starting transfers between devices, from_behind(): lax.ppermute(value, axis, [(source, source + steps) for source in range(f...  17.3 us
    reshape x1, local copies, waits for them, and re-layouts, local(): down_whole = jnp.concatenate(val2, 1)  13.8 us
  transfers between devices with their start and end apart: 12, of which 6 were waited for; matrix products, arithmetic and copies ran while one was open for 16% of the time, Pallas kernels for 0%

profile of v1, /device:TPU:0, one launch (start us, length us, event | category | flops | bytes accessed | tf_op | source)
XLA Modules:
  0.0 600.7 jit_solution(12397288756124246646)
XLA Ops:
  6.5 0.9 slice.219
  7.4 0.8 slice.220
  8.2 4.9 collective-permute-start
  13.1 0.7 reshape.164
  13.9 0.8 fusion.129
  15.4 0.9 slice_convert_fusion.3
  16.6 1.2 copy.126
  18.6 1.2 divide_multiply_fusion
  19.8 1.9 copy.124
  21.7 1.6 maximum_convert_fusion.1
  23.4 2.4 divide_multiply_fusion.1
  25.7 0.6 convolution_add_fusion.1
  26.4 1.3 fusion.44
  29.3 1.7 convolution_add_fusion.3
  31.1 2.4 fusion.43
  33.5 1.1 slice_bitcast_fusion.7
  34.7 2.8 tile.8
  37.5 6.0 all-to-all-start
  43.6 1.8 exp.125
  45.3 1.0 copy.136
  46.3 0.8 exp.120
  47.3 0.8 exp.141
  48.5 2.3 reduce-window.6
  50.9 1.0 copy.139
  52.2 1.1 copy.153
  53.7 125.0 %all-gather.5 = bf16[16,4,4]{2,1,0:T(4,128)(2,1)S(1)} all-gather(bf16[1,4,4]{2,1,0:T(4,128)(2,1)S(1)} %get-tuple-element.151), channel_id=2, replica_groups=mesh['sp'=16,'tp'=2] {'sp'}, dimensions={0}, use_global_device_ids=true | all-gather | bytes 544 | tf_op jit(solution)/shard_map/all_gather | solution.py:25
  178.7 77.4 %all-gather.6 = bf16[16,4,4]{2,1,0:T(4,128)(2,1)S(1)} all-gather(bf16[1,4,4]{2,1,0:T(4,128)(2,1)S(1)} %get-tuple-element.150), channel_id=4, replica_groups=mesh['sp'=16,'tp'=2] {'sp'}, dimensions={0}, use_global_device_ids=true | all-gather | bytes 544 | tf_op jit(solution)/shard_map/all_gather | solution.py:25
  256.3 0.6 fusion.120
  256.9 0.6 fusion.123
  260.5 0.6 fusion.40
  261.1 2.2 fusion.36
  263.3 3.0 fusion.38
  266.3 2.9 fusion.32
  269.2 3.0 fusion.34
  272.5 2.2 fusion.24
  274.7 1.0 fusion.22
  275.8 1.6 pad_maximum_fusion
  277.4 2.0 copy.154
  279.4 0.8 multiply_reduce_fusion
  280.2 2.5 psum.7
  282.6 7.0 %fusion.6 = bf16[2048,256]{0,1:T(8,128)(2,1)} fusion(bf16[2048,2048]{1,0:T(8,128)(2,1)} %param.28, f32[2048]{0:T(1024)S(1)} %copy-done.18, f32[256]{0:T(256)S(1)} %add_rsqrt_fusion.1, f32[256,2048]{1,0:T(8,128)S(1)} %copy.154, bf16[256,2048]{1,0:T(8,128)(2,1)S(1)} %copy-done.5), kind=kOutput, calls=%fused_computation.24 | convolution fusion | flops 2152726528 | bytes 12592128 | tf_op jit(solution)/shard_map/dot_general | solution.py:206
  289.7 1.3 copy.123
  291.0 36.7 %reduce-scatter.3.cloned.1.call-done = bf16[1024,256]{0,1:T(8,128)(2,1)} async-done(((bf16[2048,256]{0,1:T(8,128)(2,1)}), bf16[1024,256]{0,1:T(8,128)(2,1)}) %reduce-scatter.3.cloned.1.call-update) | async-done | bytes 524304 | tf_op jit(solution)/shard_map/reduce_scatter | solution.py:205
  327.7 2.0 add_convert_fusion.1
  330.5 2.8 tile.20
  333.4 6.9 %all-to-all-start.1 = ((bf16[16,128,1280]{2,1,0:T(8,128)(2,1)}), bf16[16,128,1280]{2,1,0:T(8,128)(2,1)}, u32[]{:S(2)}, u32[]{:S(2)}) async-start(bf16[16,128,1280]{2,1,0:T(8,128)(2,1)} %bitcast.264), calls=%async_computation.2 | async-start | bytes 10485760 | tf_op jit(solution)/shard_map/all_to_all | solution.py:233
  340.4 1.5 fusion.12
  341.9 1.5 fusion.14
  343.5 1.9 collective-permute-start.1
  345.4 39.2 %collective-permute-done.1 = bf16[2048,256]{0,1:T(8,128)(2,1)S(1)} collective-permute-done((bf16[2048,256]{0,1:T(8,128)(2,1)S(1)}, bf16[2048,256]{0,1:T(8,128)(2,1)S(1)}, u32[]{:S(2)}, u32[]{:S(2)}) %collective-permute-start.1) | collective-permute-done | bytes 1048608 | tf_op jit(solution)/shard_map/ppermute | solution.py:45
  384.6 5.8 fusion.2
  390.3 90.7 %all-to-all-done.1 = bf16[16,128,1280]{2,1,0:T(8,128)(2,1)} async-done(((bf16[16,128,1280]{2,1,0:T(8,128)(2,1)}), bf16[16,128,1280]{2,1,0:T(8,128)(2,1)}, u32[]{:S(2)}, u32[]{:S(2)}) %all-to-all-start.1) | async-done | bytes 5242912 | tf_op jit(solution)/shard_map/all_to_all | solution.py:233
  481.0 6.7 %fusion.3 = bf16[1,1280,512]{1,2,0:T(8,128)(2,1)S(1)} fusion(bf16[2048,1280]{1,0:T(8,128)(2,1)} %bitcast.75, bf16[2048,256]{0,1:T(8,128)(2,1)} %copy-done.17, bf16[2048,256]{0,1:T(8,128)(2,1)} %copy-done.7, pred[]{:T(512)S(6)} %eq.5), kind=kOutput, calls=%fused_computation.12 | convolution fusion | flops 2694447104 | bytes 8650753 | tf_op jit(solution)/shard_map/dot_general | solution.py:79
  487.7 12.4 %collective-permute-start.2 = (bf16[2,1280,2]{1,2,0:T(2,128)(2,1)S(1)}, bf16[2,1280,2]{1,2,0:T(2,128)(2,1)S(1)}, u32[]{:S(2)}, u32[]{:S(2)}) collective-permute-start(bf16[2,1280,2]{1,2,0:T(2,128)(2,1)S(1)} %pad_maximum_fusion.4), channel_id=1, source_target_pairs={{0,4},{2,6},{4,8},{6,10},{8,12},{10,14},{12,16},{14,18},{16,20},{1... | collective-permute-start | bytes 30728 | tf_op jit(solution)/shard_map/ppermute | solution.py:19
  500.2 1.2 collective-permute-done.2
  502.0 1.6 fusion
  503.6 0.8 fusion.5
  504.4 0.9 collective-permute-start.3
  505.3 57.0 %all-gather.18.cloned.1.call-done = bf16[40960,128]{1,0:T(8,128)(2,1)} async-done(((bf16[2560,128]{1,0:T(8,128)(2,1)}), bf16[40960,128]{1,0:T(8,128)(2,1)}) %all-gather.18.cloned.1.call-update) | async-done | bytes 10485776 | tf_op jit(solution)/shard_map/all_gather | solution.py:258
  562.4 13.8 %copy.155 = bf16[2560,16,128]{0,2,1:T(8,128)(2,1)} copy(bf16[2560,16,128]{2,0,1:T(8,128)(2,1)} %bitcast.279) | data formatting | bytes 20971520 | tf_op jit(solution)/shard_map/reshape | solution.py:259
  576.2 7.9 %fusion.7 = bf16[2048,256]{0,1:T(8,128)(2,1)} fusion(bf16[2560,2048]{0,1:T(8,128)(2,1)} %bitcast.280, bf16[1280,256]{0,1:T(8,128)(2,1)S(1)} %collective-permute-done.3, bf16[1280,256]{0,1:T(8,128)(2,1)S(1)} %get-tuple-element.121, pred[]{:T(512)S(6)} %eq.5), kind=kOutput, calls=%fused_computation.25 | convolution fusion | flops 2690777088 | bytes 12845057 | tf_op jit(solution)/shard_map/dot_general | solution.py:79
  584.1 7.3 %reduce-scatter.5.cloned.1.call-done = bf16[1024,256]{0,1:T(8,128)(2,1)} async-done(((bf16[2048,256]{0,1:T(8,128)(2,1)}), bf16[1024,256]{0,1:T(8,128)(2,1)}) %reduce-scatter.5.cloned.1.call-update) | async-done | bytes 524304 | tf_op jit(solution)/shard_map/reduce_scatter | solution.py:260
  591.4 1.2 add_convert_fusion
  592.6 1.0 copy.156
  (124 shorter events, 9.8 us)
Async XLA Ops:
  6.5 10.0 %copy-start.8 = (bf16[256,1536]{1,0:T(8,128)(2,1)S(1)}, bf16[256,1536]{1,0:T(8,128)(2,1)}, u32[]{:S(2)}) copy-start(bf16[256,1536]{1,0:T(8,128)(2,1)} %param.21) | copy-start | bytes 2359300
  6.5 10.0 %copy-start.13 = (bf16[4,1536]{1,0:T(4,128)(2,1)S(1)}, bf16[4,1536]{1,0:T(4,128)(2,1)}, u32[]{:S(2)}) copy-start(bf16[4,1536]{1,0:T(4,128)(2,1)} %param.26) | copy-start | bytes 36868
  6.5 265.7 %all-gather.16.cloned.1.call-start = ((), (), s32[]{:S(2)}) async-start(), calls=%async_computation.8 | async-start | bytes 4456448 | tf_op jit(solution)/shard_map/all_gather | solution.py:25
  8.2 9.8 %collective-permute-start = (bf16[3,3584]{1,0:T(4,128)(2,1)S(1)}, bf16[3,3584]{1,0:T(4,128)(2,1)S(1)}, u32[]{:S(2)}, u32[]{:S(2)}) collective-permute-start(bf16[3,3584]{1,0:T(4,128)(2,1)S(1)} %pad_maximum_fusion.3), channel_id=1, source_target_pairs={{0,2},{2,4},{4,6},{6,8},{8,10},{10,12},{12,14},{14,16},{16,18},{18... | collective-permute-start | bytes 64520 | tf_op jit(solution)/shard_map/ppermute | solution.py:19
  15.2 3.0 copy-start.4
  23.4 2.4 copy-start
  27.7 244.5 %all-gather.14.cloned.1.call-start = ((), (), s32[]{:S(2)}) async-start(), calls=%async_computation.7 | async-start | bytes 4456448 | tf_op jit(solution)/shard_map/all_gather | solution.py:25
  28.6 0.7 copy-start.3
  37.5 293.0 %all-to-all-start = ((bf16[16,128,1280]{2,1,0:T(8,128)(2,1)}), bf16[16,128,1280]{2,1,0:T(8,128)(2,1)}, u32[]{:S(2)}, u32[]{:S(2)}) async-start(bf16[16,128,1280]{2,1,0:T(8,128)(2,1)} %bitcast.263), calls=%async_computation.1 | async-start | bytes 10485760 | tf_op jit(solution)/shard_map/all_to_all | solution.py:232
  43.5 4.9 copy-start.12
  43.5 8.5 %copy-start.16 = (f32[32]{0:T(128)S(1)}, f32[32]{0:T(128)}, u32[]{:S(2)}) copy-start(f32[32]{0:T(128)} %param.24) | copy-start | bytes 388
  43.5 284.2 %reduce-scatter.3.cloned.1.call-start = ((), (), s32[]{:S(2)}) async-start(), calls=%async_computation.4 | async-start | bytes 1572864 | tf_op jit(solution)/shard_map/reduce_scatter | solution.py:205
  47.3 4.8 copy-start.6
  258.7 2.4 copy-start.1
  272.5 2.2 copy-start.10
  272.5 2.2 copy-start.11
  277.4 2.0 copy-start.5
  279.4 3.3 copy-start.18
  289.6 40.7 %copy-start.9 = (bf16[128,2560]{1,0:T(8,128)(2,1)S(1)}, bf16[128,2560]{1,0:T(8,128)(2,1)}, u32[]{:S(2)}) copy-start(bf16[128,2560]{1,0:T(8,128)(2,1)} %param.31) | copy-start | bytes 1966084
  289.6 50.7 %all-gather.12.cloned.1.call-start = ((), (), s32[]{:S(2)}) async-start(), calls=%async_computation.5 | async-start | bytes 1572864 | tf_op jit(solution)/shard_map/all_gather | solution.py:214
  329.8 232.6 %all-gather.18.cloned.1.call-start = ((), (), s32[]{:S(2)}) async-start(), calls=%async_computation.9 | async-start | bytes 11141120 | tf_op jit(solution)/shard_map/all_gather | solution.py:258
  333.3 8.6 %copy-start.14 = (f32[2048]{0:T(1024)S(1)}, f32[2048]{0:T(1024)}, u32[]{:S(2)}) copy-start(f32[2048]{0:T(1024)} %param.29) | copy-start | bytes 24580
  333.4 147.7 %all-to-all-start.1 = ((bf16[16,128,1280]{2,1,0:T(8,128)(2,1)}), bf16[16,128,1280]{2,1,0:T(8,128)(2,1)}, u32[]{:S(2)}, u32[]{:S(2)}) async-start(bf16[16,128,1280]{2,1,0:T(8,128)(2,1)} %bitcast.264), calls=%async_computation.2 | async-start | bytes 10485760 | tf_op jit(solution)/shard_map/all_to_all | solution.py:233
  340.3 251.1 %reduce-scatter.5.cloned.1.call-start = ((), (), s32[]{:S(2)}) async-start(), calls=%async_computation.6 | async-start | bytes 1572864 | tf_op jit(solution)/shard_map/reduce_scatter | solution.py:260
  343.4 46.9 %copy-start.7 = (bf16[2048,256]{0,1:T(8,128)(2,1)}, bf16[2048,256]{0,1:T(8,128)(2,1)S(1)}, u32[]{:S(2)}) copy-start(bf16[2048,256]{0,1:T(8,128)(2,1)S(1)} %fusion.14) | copy-start | bytes 3145732
  343.5 41.1 %collective-permute-start.1 = (bf16[2048,256]{0,1:T(8,128)(2,1)S(1)}, bf16[2048,256]{0,1:T(8,128)(2,1)S(1)}, u32[]{:S(2)}, u32[]{:S(2)}) collective-permute-start(bf16[2048,256]{0,1:T(8,128)(2,1)S(1)} %fusion.14), channel_id=1, source_target_pairs={{0,2},{2,0},{4,6},{6,4},{8,10},{10,8},{12,14},{14,12},{16,18},{18,... | collective-permute-start | bytes 3145736 | tf_op jit(solution)/shard_map/ppermute | solution.py:45
  384.5 5.8 copy-start.17
  487.7 12.5 %copy-start.15 = (bf16[2,3,2560]{2,0,1:T(2,128)(2,1)S(1)}, bf16[2,3,2560]{2,0,1:T(2,128)(2,1)}, u32[]{:S(2)}) copy-start(bf16[2,3,2560]{2,0,1:T(2,128)(2,1)} %param.32) | copy-start | bytes 92164
  487.7 13.7 %collective-permute-start.2 = (bf16[2,1280,2]{1,2,0:T(2,128)(2,1)S(1)}, bf16[2,1280,2]{1,2,0:T(2,128)(2,1)S(1)}, u32[]{:S(2)}, u32[]{:S(2)}) collective-permute-start(bf16[2,1280,2]{1,2,0:T(2,128)(2,1)S(1)} %pad_maximum_fusion.4), channel_id=1, source_target_pairs={{0,4},{2,6},{4,8},{6,10},{8,12},{10,14},{12,16},{14,18},{16,20},{1... | collective-permute-start | bytes 30728 | tf_op jit(solution)/shard_map/ppermute | solution.py:19
  504.4 71.7 %collective-permute-start.3 = (bf16[1280,256]{0,1:T(8,128)(2,1)S(1)}, bf16[1280,256]{0,1:T(8,128)(2,1)S(1)}, u32[]{:S(2)}, u32[]{:S(2)}) collective-permute-start(bf16[1280,256]{0,1:T(8,128)(2,1)S(1)} %get-tuple-element.122), channel_id=1, source_target_pairs={{0,2},{2,0},{4,6},{6,4},{8,10},{10,8},{12,14},{14,12},{16,18},{18,... | collective-permute-start | bytes 1966088 | tf_op jit(solution)/shard_map/ppermute | solution.py:45
  576.2 15.2 %copy-start.2 = (bf16[1024,256]{0,1:T(8,128)(2,1)S(1)}, bf16[1024,256]{0,1:T(8,128)(2,1)}, u32[]{:S(2)}) copy-start(bf16[1024,256]{0,1:T(8,128)(2,1)} %add_convert_fusion.1) | copy-start | bytes 1572868
Sparse Core Ops, SparseCore 0:
  27.9 156.5 all-gather.15
  187.3 74.8 all-gather.13
  289.8 37.9 reduce-scatter.2
  329.9 10.1 all-gather.11
  342.7 219.6 all-gather.17
  584.2 7.0 reduce-scatter.4
